TPU v7x, 32 devices: a whole 2x2x4 slice. The times are simulated.
32 devices in a mesh: ep: 8 (over z, core), tp: 4 (over y, x).
Axes of the slice: x: 2, y: 2, z: 4, core: 2. Of those that a mesh axis runs over, the one named last changes fastest.
Arguments:
- tokens: bfloat16 [1024, 2048], P('ep', 'tp'), may hold values from -540 to 540
- expert_ids: int32 [1024, 2], P('ep'), may hold values from 0 to 7, all different within a row; in each aligned block of 128 rows (0 to 127, 128 to 255, ...) at most 64 rows name the same one
- gate_weights: float32 [1024, 2], P('ep'), may hold values from 0.1 to 1
- gain_in: float32 [2048], P('tp'), may hold values from 0.1 to 1.9
- gain_out: float32 [2048], P('tp'), may hold values from 0.1 to 1.9
- w_gate: bfloat16 [8, 2048, 8192], P('ep', None, 'tp'), may hold values from -0.125 to 0.125
- w_up: bfloat16 [8, 2048, 8192], P('ep', None, 'tp'), may hold values from -0.125 to 0.125
- w_down: bfloat16 [8, 8192, 2048], P('ep', 'tp'), may hold values from -0.397747564 to 0.397747564
Outputs:
- mixed: bfloat16 [1024, 2048], P('ep', 'tp')
Inputs may be any that keep to these rules, and one draw needn't show every extreme that they name: `expert_ids`: each row names 2 different experts. In the rows of one index of ep (aligned blocks of 128 rows) no expert is named by more than 64 rows, a bound that some block reaches.
All inputs are finite; a program needn't handle non-finite values.
Results may differ from a plain program's by a relative error of at most 0.018.
Values may be sent and summed in bfloat16 or wider, within the bound.
A program may use at most 64 MiB of HBM per device.

v0:
```python
import jax
import jax.numpy as jnp
from jax import lax
from jax.sharding import PartitionSpec as P

TOP = 2


NORM_EPS = 1e-06


def on_device(tokens, expert_ids, gate_weights, gain_in, gain_out, w_gate, w_up, w_down):
    count_tp = lax.axis_size("tp")
    count_ep = lax.axis_size("ep")
    tok_rows = tokens.shape[0]
    model_width = tokens.shape[1] * count_tp
    capacity = 2 * TOP * tok_rows // count_ep
    values = tokens.astype(jnp.float32)
    squares = lax.psum(jnp.sum(values * values, axis=1), "tp")
    normed = (values * lax.rsqrt(squares[:, None] / model_width + NORM_EPS) * gain_in).astype(
        jnp.bfloat16
    )
    flat_ids = expert_ids.reshape(-1)
    one_hot = (flat_ids[:, None] == jnp.arange(count_ep, dtype=jnp.int32)[None, :]).astype(
        jnp.int32
    )
    earlier = jnp.cumsum(one_hot, axis=0) - 1
    slot_index = jnp.sum(one_hot * earlier, axis=1)
    places = (flat_ids * capacity + slot_index).reshape(tok_rows, TOP)
    slot_rows = jnp.arange(count_ep * capacity, dtype=jnp.int32)
    picker = jnp.sum((slot_rows[:, None, None] == places[None, :, :]).astype(jnp.bfloat16), axis=2)
    gate_w = w_gate[0]
    up_w = w_up[0]
    down_w = w_down[0]
    outgoing = jnp.dot(picker, normed, preferred_element_type=jnp.float32).astype(jnp.bfloat16)
    arrived = lax.all_to_all(outgoing, "ep", split_axis=0, concat_axis=0, tiled=True)
    shard_part = lax.all_gather(arrived, "tp", axis=1, tiled=True)
    gate_part = jnp.dot(shard_part, gate_w, preferred_element_type=jnp.float32)
    up_part = jnp.dot(shard_part, up_w, preferred_element_type=jnp.float32)
    hidden = (jax.nn.silu(gate_part) * up_part).astype(jnp.bfloat16)
    partial_value = lax.optimization_barrier(
        jnp.dot(hidden, down_w, preferred_element_type=jnp.float32).astype(jnp.bfloat16)
    )
    summed = lax.psum_scatter(
        partial_value.astype(jnp.float32).astype(jnp.bfloat16),
        "tp",
        scatter_dimension=1,
        tiled=True,
    ).astype(jnp.float32)
    returned = lax.all_to_all(
        summed.astype(jnp.bfloat16), "ep", split_axis=0, concat_axis=0, tiled=True
    ).astype(summed.dtype)
    combined = jnp.sum(gate_weights[:, :, None] * returned[places], axis=1)
    squares_out = lax.psum(jnp.sum(combined * combined, axis=1), "tp")
    scale = lax.rsqrt(squares_out[:, None] / model_width + NORM_EPS)
    return (combined * scale * gain_out).astype(jnp.bfloat16)


def solution(mesh):
    placed = (
        P("ep", "tp"),
        P("ep", None),
        P("ep", None),
        P("tp"),
        P("tp"),
        P("ep", None, "tp"),
        P("ep", None, "tp"),
        P("ep", "tp", None),
    )
    return jax.shard_map(
        on_device, mesh=mesh, in_specs=placed, out_specs=P("ep", "tp"), check_vma=False
    )
```

profile of v0, /device:TPU:0, one launch (start us, length us, event | category | flops | bytes accessed | tf_op | source)
XLA Modules:
  0.0 177.8 jit_solution(11088431185920672371)
XLA Ops:
  6.5 0.8 copy.23
  7.3 0.1 eq.43
  7.5 0.1 eq.39
  7.6 0.6 reduce-window.6
  8.2 0.2 slice_reduce_fusion
  8.5 0.1 fusion.24
  8.6 0.1 reduce_sum.51
  8.7 0.1 copy.25
  8.8 0.7 compare_select_fusion
  9.5 0.1 fusion.20
  9.5 1.0 fusion.17
  10.6 11.4 %psum.14 = f32[128]{0:T(128)S(1)} all-reduce(f32[128]{0:T(128)S(1)} %fusion.17), channel_id=1, replica_groups=mesh['ep'=8,'tp'=4] {'tp'}, use_global_device_ids=true, to_apply=%region_5.6 | all-reduce | flops 128 | bytes 1024 | tf_op jit(solution)/shard_map/psum | solution.py:19
  22.0 1.3 convolution_convert_fusion
  23.2 20.1 %all_to_all.21 = bf16[8,64,512]{2,1,0:T(8,128)(2,1)} all-to-all(bf16[8,64,512]{2,1,0:T(8,128)(2,1)S(1)} %bitcast.33), channel_id=1, replica_groups=mesh['ep'=8,'tp'=4] {'ep'}, dimensions={0} | all-to-all | bytes 1048576 | tf_op jit(solution)/shard_map/all_to_all | solution.py:36
  43.3 0.0 all-gather.2.cloned.1.call-update
  43.4 0.0 reduce-scatter.2.cloned.1.call-start
  43.4 32.2 %all-gather.2.cloned.1.call-done = bf16[512,2048]{1,0:T(8,128)(2,1)} async-done(((bf16[512,512]{1,0:T(8,128)(2,1)}), bf16[512,2048]{1,0:T(8,128)(2,1)}) %all-gather.2.cloned.1.call-update) | async-done | bytes 2097168 | tf_op jit(solution)/shard_map/all_gather | solution.py:37
  75.6 10.6 %fusion.4 = f32[512,2048]{1,0:T(8,128)} fusion(bf16[512,2048]{1,0:T(8,128)(2,1)} %all-gather.2.cloned.1.call-done, bf16[1,2048,2048]{2,1,0:T(8,128)(2,1)} %param.13), kind=kOutput, calls=%fused_computation.5 | convolution fusion | flops 4294967296 | bytes 14680064 | tf_op jit(solution)/shard_map/dot_general | solution.py:38
  86.2 17.5 %fusion.10 = bf16[512,2048]{1,0:T(8,128)(2,1)} fusion(bf16[1,2048,2048]{2,1,0:T(8,128)(2,1)} %param.15, f32[512,2048]{1,0:T(8,128)} %fusion.4, bf16[512,2048]{1,0:T(8,128)(2,1)S(1)} %copy-done.2, bf16[1,2048,2048]{2,1,0:T(8,128)(2,1)} %param.14), kind=kOutput, calls=%fused_computation.8 | convolution fusion | flops 8597274624 | bytes 25165824 | tf_op jit(solution)/shard_map/dot_general | solution.py:42
  103.7 35.3 %reduce-scatter.2.cloned.1.call-done = bf16[512,512]{1,0:T(8,128)(2,1)} async-done(((bf16[512,2048]{1,0:T(8,128)(2,1)}), bf16[512,512]{1,0:T(8,128)(2,1)}) %reduce-scatter.2.cloned.1.call-update) | async-done | bytes 524304 | tf_op jit(solution)/shard_map/reduce_scatter | solution.py:44
  139.0 4.6 %all-to-all-start.1 = ((bf16[8,64,512]{2,1,0:T(8,128)(2,1)}), bf16[8,64,512]{2,1,0:T(8,128)(2,1)S(1)}, u32[]{:S(2)}, u32[]{:S(2)}) async-start(bf16[8,64,512]{2,1,0:T(8,128)(2,1)} %bitcast.34), calls=%async_computation.2 | async-start | bytes 1048576 | tf_op jit(solution)/shard_map/all_to_all | solution.py:50
  143.6 0.1 copy.26
  143.8 0.1 reshape.49
  143.9 0.1 copy.22
  144.0 14.9 %all-to-all-done.1 = bf16[8,64,512]{2,1,0:T(8,128)(2,1)S(1)} async-done(((bf16[8,64,512]{2,1,0:T(8,128)(2,1)}), bf16[8,64,512]{2,1,0:T(8,128)(2,1)S(1)}, u32[]{:S(2)}, u32[]{:S(2)}) %all-to-all-start.1) | async-done | bytes 524320 | tf_op jit(solution)/shard_map/all_to_all | solution.py:50
  159.0 0.1 bitcast_convert_fusion
  159.1 1.0 gather_fusion
  160.1 0.3 reshape.48
  160.4 0.7 multiply_reduce_fusion
  161.1 0.1 multiply_reduce_fusion.1
  161.2 8.9 %psum.15 = f32[128]{0:T(128)S(1)} all-reduce(f32[128]{0:T(128)S(1)} %multiply_reduce_fusion.1), channel_id=1, replica_groups=mesh['ep'=8,'tp'=4] {'tp'}, use_global_device_ids=true, to_apply=%region_9.10 | all-reduce | flops 128 | bytes 1024 | tf_op jit(solution)/shard_map/psum | solution.py:54
  170.2 0.8 multiply_convert_fusion.1
  (14 shorter events, 0.1 us)
Async XLA Ops:
  6.5 69.1 %all-gather.2.cloned.1.call-start = ((), (), s32[]{:S(2)}) async-start(), calls=%async_computation.3 | async-start | bytes 2621440 | tf_op jit(solution)/shard_map/all_gather | solution.py:37
  43.4 95.7 %reduce-scatter.2.cloned.1.call-start = ((), (), s32[]{:S(2)}) async-start(), calls=%async_computation.4 | async-start | bytes 2621440 | tf_op jit(solution)/shard_map/reduce_scatter | solution.py:44
  75.6 10.6 %copy-start.2 = (bf16[512,2048]{1,0:T(8,128)(2,1)S(1)}, bf16[512,2048]{1,0:T(8,128)(2,1)}, u32[]{:S(2)}) copy-start(bf16[512,2048]{1,0:T(8,128)(2,1)} %all-gather.2.cloned.1.call-done) | copy-start | bytes 6291460
  86.2 57.7 %copy-start.1 = (f32[128,2]{0,1:T(2,128)S(1)}, f32[128,2]{0,1:T(2,128)}, u32[]{:S(2)}) copy-start(f32[128,2]{0,1:T(2,128)} %param.10) | copy-start | bytes 3076
  139.0 19.9 %all-to-all-start.1 = ((bf16[8,64,512]{2,1,0:T(8,128)(2,1)}), bf16[8,64,512]{2,1,0:T(8,128)(2,1)S(1)}, u32[]{:S(2)}, u32[]{:S(2)}) async-start(bf16[8,64,512]{2,1,0:T(8,128)(2,1)} %bitcast.34), calls=%async_computation.2 | async-start | bytes 1048576 | tf_op jit(solution)/shard_map/all_to_all | solution.py:50
  144.0 26.2 %copy-start = (f32[512]{0:T(512)S(1)}, f32[512]{0:T(512)}, u32[]{:S(2)}) copy-start(f32[512]{0:T(512)} %param.12) | copy-start | bytes 6148
Sparse Core Ops, SparseCore 0:
  43.5 32.0 all-gather.1
  103.8 35.1 reduce-scatter.1
where the time goes:
time: 178 us
  waiting for transfers between devices  82.5 us (46%)
  blocking collectives  40.4 us (23%)
  matrix products  29.3 us (16%)
  between operations  13.5 us (8%)
  starting transfers between devices  4.65 us (3%)
  other arithmetic  4.23 us (2%)
  local copies, waits for them, and re-layouts  3.14 us (2%)
    reduce_scatter x1, waiting for transfers between devices, on_device(): lax.psum_scatter(partial_value.astype(jnp.float32).astype(jnp.bfloat16),...  35.3 us
    all_gather x1, waiting for transfers between devices, on_device(): shard_part = lax.all_gather(arrived, 'tp', axis=1, tiled=True)  32.2 us
    all_to_all x1, blocking collectives, on_device(): lax.all_to_all(outgoing, 'ep', split_axis=0, concat_axis=0, tiled=True)  20.1 us
    dot_general x1, matrix products, on_device(): jnp.dot(hidden, down_w, preferred_element_type=jnp.float32)  17.5 us
    all_to_all x1, waiting for transfers between devices, on_device(): lax.all_to_all(summed.astype(jnp.bfloat16), 'ep', split_axis=0, concat_ax...  14.9 us
    psum x1, blocking collectives, on_device(): squares = lax.psum(jnp.sum(values * values, axis=1), 'tp')  11.4 us
    dot_general x1, matrix products, on_device(): gate_part = jnp.dot(shard_part, gate_w, preferred_element_type=jnp.float32)  10.6 us
    psum x1, blocking collectives, on_device(): squares_out = lax.psum(jnp.sum(combined * combined, axis=1), 'tp')  8.94 us
  transfers between devices with their start and end apart: 3, of which 3 were waited for; matrix products, arithmetic and copies ran while one was open for 0% of the time, Pallas kernels for 0%

commit v1 on v0

--- a/solution.py
+++ b/solution.py
@@ -1,6 +1,8 @@
 import jax
 import jax.numpy as jnp
 from jax import lax
+from jax.experimental import pallas as pl
+from jax.experimental.pallas import tpu as pltpu
 from jax.sharding import PartitionSpec as P
 
 TOP = 2
@@ -9,7 +11,7 @@
 NORM_EPS = 1e-06
 
 
-def on_device(tokens, expert_ids, gate_weights, gain_in, gain_out, w_gate, w_up, w_down):
+def on_device_plain(tokens, expert_ids, gate_weights, gain_in, gain_out, w_gate, w_up, w_down):
     count_tp = lax.axis_size("tp")
     count_ep = lax.axis_size("ep")
     tok_rows = tokens.shape[0]
@@ -56,6 +58,255 @@
     return (combined * scale * gain_out).astype(jnp.bfloat16)
 
 
+MESH = pl.DeviceIdType.MESH
+
+
+def greet_everyone(count, me, count_tp):
+    barrier = pltpu.get_barrier_semaphore()
+
+    @pl.loop(1, count)
+    def _(step):
+        peer = lax.rem(me + step, count)
+        pl.semaphore_signal(
+            barrier, inc=1, device_id=(peer // count_tp, lax.rem(peer, count_tp)),
+            device_id_type=MESH,
+        )
+
+    pl.semaphore_wait(barrier, count - 1)
+
+
+def dispatch_kernel(
+    count_ep, count_tp, picked, gain, rows_out, gain_out,
+    send_sem, recv_sem, gain_send, gain_recv, own_sem,
+):
+    ep, tp = lax.axis_index("ep"), lax.axis_index("tp")
+    me, count = ep * count_tp + tp, count_ep * count_tp
+    cap, width = picked.shape[1], picked.shape[2]
+
+    def spot(owner):
+        place_rows = pl.ds(pl.multiple_of((owner // count_tp) * cap, cap), cap)
+        place_cols = pl.ds(pl.multiple_of(lax.rem(owner, count_tp) * width, width), width)
+        return rows_out.at[place_rows, place_cols]
+
+    def gain_spot(owner_tp):
+        return gain_out.at[:, pl.ds(pl.multiple_of(owner_tp * width, width), width)]
+
+    def rows_copy(peer, owner):
+        return pltpu.make_async_remote_copy(
+            src_ref=picked.at[peer // count_tp],
+            dst_ref=spot(owner),
+            send_sem=send_sem.at[peer],
+            recv_sem=recv_sem.at[owner],
+            device_id=(peer // count_tp, lax.rem(peer, count_tp)),
+            device_id_type=MESH,
+        )
+
+    def gain_copy(peer_tp, owner_tp):
+        return pltpu.make_async_remote_copy(
+            src_ref=gain,
+            dst_ref=gain_spot(owner_tp),
+            send_sem=gain_send.at[peer_tp],
+            recv_sem=gain_recv.at[owner_tp],
+            device_id=(ep, peer_tp),
+            device_id_type=MESH,
+        )
+
+    own_rows = pltpu.make_async_copy(picked.at[ep], spot(me), own_sem.at[0])
+    own_gain = pltpu.make_async_copy(gain, gain_spot(tp), own_sem.at[1])
+    own_rows.start()
+    own_gain.start()
+    greet_everyone(count, me, count_tp)
+
+    @pl.loop(1, count)
+    def _(step):
+        rows_copy(lax.rem(me + step, count), me).start()
+
+    for step in range(1, count_tp):
+        gain_copy(lax.rem(tp + step, count_tp), tp).start()
+    own_rows.wait()
+    own_gain.wait()
+
+    @pl.loop(1, count)
+    def _(step):
+        peer = lax.rem(me + step, count)
+        copy = rows_copy(peer, peer)
+        copy.wait_send()
+        copy.wait_recv()
+
+    for step in range(1, count_tp):
+        peer_tp = lax.rem(tp + step, count_tp)
+        copy = gain_copy(peer_tp, peer_tp)
+        copy.wait_send()
+        copy.wait_recv()
+
+
+def dispatch(count_ep, count_tp, picked, gain):
+    cap, width = picked.shape[1:]
+    count = count_ep * count_tp
+    return pl.pallas_call(
+        lambda *refs: dispatch_kernel(count_ep, count_tp, *refs),
+        out_shape=(
+            jax.ShapeDtypeStruct((count_ep * cap, count_tp * width), picked.dtype),
+            jax.ShapeDtypeStruct((gain.shape[0], count_tp * width), gain.dtype),
+        ),
+        in_specs=[pl.BlockSpec(memory_space=pltpu.VMEM)] * 2,
+        out_specs=[pl.BlockSpec(memory_space=pltpu.VMEM)] * 2,
+        scratch_shapes=[
+            pltpu.SemaphoreType.DMA((count,)),
+            pltpu.SemaphoreType.DMA((count,)),
+            pltpu.SemaphoreType.DMA((count_tp,)),
+            pltpu.SemaphoreType.DMA((count_tp,)),
+            pltpu.SemaphoreType.DMA((2,)),
+        ],
+        compiler_params=pltpu.CompilerParams(collective_id=0, has_side_effects=True),
+    )(picked, gain)
+
+
+def return_kernel(
+    count_ep, count_tp, partial, first_pick, second_pick, weights, gain, mixed,
+    landed, stats, send_sem, recv_sem, stat_send, stat_recv, own_sem,
+):
+    ep, tp = lax.axis_index("ep"), lax.axis_index("tp")
+    me, count = ep * count_tp + tp, count_ep * count_tp
+    cap, width = partial.shape[0] // count_ep, partial.shape[1] // count_tp
+
+    def source(owner):
+        from_rows = pl.ds(pl.multiple_of((owner // count_tp) * cap, cap), cap)
+        from_cols = pl.ds(pl.multiple_of(lax.rem(owner, count_tp) * width, width), width)
+        return partial.at[from_rows, from_cols]
+
+    def spot(owner):
+        place_rows = pl.ds(pl.multiple_of((owner // count_tp) * cap, cap), cap)
+        return landed.at[lax.rem(owner, count_tp), place_rows, :]
+
+    def rows_copy(peer, owner):
+        return pltpu.make_async_remote_copy(
+            src_ref=source(peer),
+            dst_ref=spot(owner),
+            send_sem=send_sem.at[peer],
+            recv_sem=recv_sem.at[owner],
+            device_id=(peer // count_tp, lax.rem(peer, count_tp)),
+            device_id_type=MESH,
+        )
+
+    def stat_copy(peer_tp, owner_tp):
+        return pltpu.make_async_remote_copy(
+            src_ref=stats.at[tp],
+            dst_ref=stats.at[owner_tp],
+            send_sem=stat_send.at[peer_tp],
+            recv_sem=stat_recv.at[owner_tp],
+            device_id=(ep, peer_tp),
+            device_id_type=MESH,
+        )
+
+    own_rows = pltpu.make_async_copy(source(me), spot(me), own_sem.at[0])
+    own_rows.start()
+    greet_everyone(count, me, count_tp)
+
+    @pl.loop(1, count)
+    def _(step):
+        rows_copy(lax.rem(me + step, count), me).start()
+
+    own_rows.wait()
+
+    @pl.loop(1, count)
+    def _(step):
+        peer = lax.rem(me + step, count)
+        copy = rows_copy(peer, peer)
+        copy.wait_send()
+        copy.wait_recv()
+
+    def picked_sum(pick):
+        total = jnp.zeros(mixed.shape, jnp.float32)
+        for part in range(count_tp):
+            total += jnp.dot(pick[...], landed[part], preferred_element_type=jnp.float32)
+        return total
+
+    combined = weights[:, 0:1] * picked_sum(first_pick) + weights[:, 1:2] * picked_sum(second_pick)
+    squares = jnp.sum(combined * combined, axis=1, keepdims=True)
+    stats[tp] = jnp.broadcast_to(squares, stats.shape[1:])
+    for step in range(1, count_tp):
+        stat_copy(lax.rem(tp + step, count_tp), tp).start()
+    for step in range(1, count_tp):
+        peer_tp = lax.rem(tp + step, count_tp)
+        copy = stat_copy(peer_tp, peer_tp)
+        copy.wait_send()
+        copy.wait_recv()
+    everything = stats[0]
+    for part in range(1, count_tp):
+        everything += stats[part]
+    scale = lax.rsqrt(everything[:, 0:1] / (count_tp * width) + NORM_EPS)
+    mixed[...] = (combined * scale * gain[...]).astype(mixed.dtype)
+
+
+def give_back(count_ep, count_tp, partial, picks, weights, gain):
+    tok_rows, width = weights.shape[0], gain.shape[1]
+    count = count_ep * count_tp
+    return pl.pallas_call(
+        lambda *refs: return_kernel(count_ep, count_tp, *refs),
+        out_shape=jax.ShapeDtypeStruct((tok_rows, width), jnp.bfloat16),
+        in_specs=[pl.BlockSpec(memory_space=pltpu.VMEM)] * 5,
+        out_specs=pl.BlockSpec(memory_space=pltpu.VMEM),
+        scratch_shapes=[
+            pltpu.VMEM((count_tp, partial.shape[0], width), jnp.bfloat16),
+            pltpu.VMEM((count_tp, tok_rows, 128), jnp.float32),
+            pltpu.SemaphoreType.DMA((count,)),
+            pltpu.SemaphoreType.DMA((count,)),
+            pltpu.SemaphoreType.DMA((count_tp,)),
+            pltpu.SemaphoreType.DMA((count_tp,)),
+            pltpu.SemaphoreType.DMA((1,)),
+        ],
+        compiler_params=pltpu.CompilerParams(collective_id=1, has_side_effects=True),
+    )(partial, picks[0], picks[1], weights, gain)
+
+
+def on_device_direct(
+    tokens, expert_ids, gate_weights, gain_in, gain_out, w_gate, w_up, w_down
+):
+    count_tp = lax.axis_size("tp")
+    count_ep = lax.axis_size("ep")
+    tok_rows, width = tokens.shape
+    model_width = width * count_tp
+    capacity = 2 * TOP * tok_rows // count_ep
+    flat_ids = expert_ids.reshape(-1)
+    experts = jnp.arange(count_ep, dtype=jnp.int32)
+    named = (expert_ids[:, :, None] == experts).astype(jnp.float32)
+    per_token = jnp.sum(named, axis=1)
+    positions = jnp.arange(tok_rows, dtype=jnp.int32)
+    before = (positions[:, None] > positions[None, :]).astype(jnp.float32)
+    earlier = jnp.dot(before, per_token, preferred_element_type=jnp.float32)
+    slot_index = jnp.sum(named * earlier[:, None, :], axis=2).astype(jnp.int32)
+    places = expert_ids * capacity + slot_index
+    slot_rows = jnp.arange(count_ep * capacity, dtype=jnp.int32)
+    picks = [
+        (places[:, k : k + 1] == slot_rows[None, :]).astype(jnp.bfloat16) for k in range(TOP)
+    ]
+    picker = (
+        (slot_rows[:, None] == places[None, :, 0]) | (slot_rows[:, None] == places[None, :, 1])
+    ).astype(jnp.bfloat16)
+    picked = jnp.dot(picker, tokens, preferred_element_type=jnp.float32).astype(jnp.bfloat16)
+    rows, gain = dispatch(
+        count_ep, count_tp, picked.reshape(count_ep, capacity, width),
+        jnp.broadcast_to(gain_in[None, :], (8, width)),
+    )
+    values = rows.astype(jnp.float32)
+    squares = jnp.sum(values * values, axis=1, keepdims=True)
+    normed = (values * lax.rsqrt(squares / model_width + NORM_EPS) * gain[0:1]).astype(
+        jnp.bfloat16
+    )
+    gate_part = jnp.dot(normed, w_gate[0], preferred_element_type=jnp.float32)
+    up_part = jnp.dot(normed, w_up[0], preferred_element_type=jnp.float32)
+    hidden = (jax.nn.silu(gate_part) * up_part).astype(jnp.bfloat16)
+    partial = jnp.dot(hidden, w_down[0], preferred_element_type=jnp.float32).astype(jnp.bfloat16)
+    return give_back(count_ep, count_tp, partial, picks, gate_weights, gain_out[None, :])
+
+
+def on_device(tokens, *others):
+    if tokens.shape[1] % 128:
+        return on_device_plain(tokens, *others)
+    return on_device_direct(tokens, *others)
+
+
 def solution(mesh):
     placed = (
         P("ep", "tp"),

time: 178 us -> 153 us (0.86)
  the two profiles are of different devices: /device:TPU:0 before, /device:TPU:9 now
where the time goes in v1:
time: 153 us
  Pallas kernels  114 us (75%)
  matrix products  29.4 us (19%)
  other arithmetic  5.01 us (3%)
  local copies, waits for them, and re-layouts  4.45 us (3%)
    pallas_call x1, Pallas kernels, give_back(): pl.pallas_call(lambda *refs: return_kernel(count_ep, count_tp, *refs), ou...  60.8 us
    pallas_call x1, Pallas kernels, dispatch(): pl.pallas_call(lambda *refs: dispatch_kernel(count_ep, count_tp, *refs),...  53.3 us
    dot_general x1, matrix products, on_device_direct(): jnp.dot(hidden, w_down[0], preferred_element_type=jnp.float32)  17.6 us
    dot_general x1, matrix products, on_device_direct(): gate_part = jnp.dot(normed, w_gate[0], preferred_element_type=jnp.float32)  10.6 us

profile of v1, /device:TPU:9, one launch (start us, length us, event | category | flops | bytes accessed | tf_op | source)
XLA Modules:
  0.0 152.9 jit_solution(4515822324083006444)
XLA Ops:
  0.0 0.0 copy-start
  0.0 0.7 convert_reduce_fusion
  0.7 0.1 fusion.28
  0.9 0.7 select_reduce_fusion
  1.6 0.7 convert_add_fusion
  2.3 0.0 copy-done
  2.3 1.1 convolution_convert_fusion
  3.4 1.3 broadcast_in_dim.4.refs_1_
  4.6 53.3 %shard_map.82 = (bf16[512,2048]{1,0:T(8,128)(2,1)}, f32[8,2048]{1,0:T(8,128)}) custom-call(bf16[8,64,512]{2,1,0:T(8,128)(2,1)} %bitcast.26, f32[8,512]{1,0:T(8,128)} %broadcast_in_dim.4.refs_1_), custom_call_target="tpu_custom_call" | custom-call | tf_op jit(solution)/shard_map/pallas_call | solution.py:146
  57.9 2.1 %fusion.6 = f32[512]{0:T(512)S(1)} fusion(bf16[512,2048]{1,0:T(8,128)(2,1)} %get-tuple-element.7), kind=kLoop, calls=%fused_computation.8 | loop fusion | flops 3145216 | bytes 2099200 | tf_op jit(solution)/shard_map/reduce_sum | solution.py:293
  60.0 0.9 slice.13
  60.8 0.0 copy-start.1
  60.8 10.6 %fusion.4 = f32[512,2048]{1,0:T(8,128)} fusion(bf16[1,2048,2048]{2,1,0:T(8,128)(2,1)} %param.13, bf16[512,2048]{1,0:T(8,128)(2,1)} %get-tuple-element.7, f32[2048]{0:T(1024)S(1)} %bitcast.27, f32[512]{0:T(512)S(1)} %add_rsqrt_fusion), kind=kOutput, calls=%fused_computation.4 | convolution fusion | flops 4299161600 | bytes 14690304 | tf_op jit(solution)/shard_map/dot_general | solution.py:297
  71.5 0.0 copy-done.1
  71.5 0.0 copy-start.2
  71.5 17.6 %fusion.13.refs_0_ = bf16[512,2048]{1,0:T(8,128)(2,1)} fusion(bf16[1,2048,2048]{2,1,0:T(8,128)(2,1)} %param.15, f32[512,2048]{1,0:T(8,128)} %fusion.4, bf16[1,2048,2048]{2,1,0:T(8,128)(2,1)} %param.14, bf16[512,2048]{1,0:T(8,128)(2,1)S(1)} %copy-done.1, f32[2048]{0:T(1024)S(1)} %bitcast.28, f32[512]{0:T(512)S(1)} %add_rsqrt_fusion), kind=kOutput, calls=%fused_computation.12 | convolution fusion | flops 8601468928 | bytes 25176064 | tf_op jit(solution)/shard_map/dot_general | solution.py:300
  89.0 0.8 fusion.24
  89.8 0.0 copy-done.2
  89.9 0.7 copy.12.refs_3_
  90.6 60.8 %shard_map.83 = bf16[128,512]{1,0:T(8,128)(2,1)} custom-call(bf16[512,2048]{1,0:T(8,128)(2,1)} %fusion.13.refs_0_, bf16[128,512]{1,0:T(8,128)(2,1)} %get-tuple-element.11.refs_1_, bf16[128,512]{1,0:T(8,128)(2,1)} %get-tuple-element.12.refs_2_, f32[128,2]{1,0:T(8,128)} %copy.12.refs_3_, f32[1,512]{1,0:T(1,128)} %bitcast.29), custom_call_target="tpu_custom_call" | custom-call | tf_op jit(solution)/shard_map/pallas_call | solution.py:245
  151.4 1.6 %copy.14 = bf16[128,512]{1,0:T(8,128)(2,1)} copy(bf16[128,512]{1,0:T(8,128)(2,1)} %shard_map.83) | data formatting | bytes 262144
  (2 shorter events, 0.0 us)
Async XLA Ops:
  0.0 2.3 %copy-start = (bf16[128,512]{1,0:T(8,128)(2,1)S(1)}, bf16[128,512]{1,0:T(8,128)(2,1)}, u32[]{:S(2)}) copy-start(bf16[128,512]{1,0:T(8,128)(2,1)} %param.8) | copy-start | bytes 393220
  60.8 10.6 %copy-start.1 = (bf16[512,2048]{1,0:T(8,128)(2,1)S(1)}, bf16[512,2048]{1,0:T(8,128)(2,1)}, u32[]{:S(2)}) copy-start(bf16[512,2048]{1,0:T(8,128)(2,1)} %get-tuple-element.7) | copy-start | bytes 6291460
  71.5 18.4 %copy-start.2 = (f32[128,2]{0,1:T(2,128)S(1)}, f32[128,2]{0,1:T(2,128)}, u32[]{:S(2)}) copy-start(f32[128,2]{0,1:T(2,128)} %param.10) | copy-start | bytes 3076

commit v2 on v1

--- a/solution.py
+++ b/solution.py
@@ -61,31 +61,27 @@
 MESH = pl.DeviceIdType.MESH
 
 
-def greet_everyone(count, me, count_tp):
+def greet(count_ep, count_tp, ep, tp):
     barrier = pltpu.get_barrier_semaphore()
-
-    @pl.loop(1, count)
-    def _(step):
-        peer = lax.rem(me + step, count)
-        pl.semaphore_signal(
-            barrier, inc=1, device_id=(peer // count_tp, lax.rem(peer, count_tp)),
-            device_id_type=MESH,
-        )
-
-    pl.semaphore_wait(barrier, count - 1)
+    for step in range(1, count_ep):
+        peer = (lax.rem(ep + step, count_ep), tp)
+        pl.semaphore_signal(barrier, inc=1, device_id=peer, device_id_type=MESH)
+    for step in range(1, count_tp):
+        peer = (ep, lax.rem(tp + step, count_tp))
+        pl.semaphore_signal(barrier, inc=1, device_id=peer, device_id_type=MESH)
+    pl.semaphore_wait(barrier, count_ep + count_tp - 2)
 
 
 def dispatch_kernel(
     count_ep, count_tp, picked, gain, rows_out, gain_out,
-    send_sem, recv_sem, gain_send, gain_recv, own_sem,
+    send_sem, recv_sem, pass_send, pass_recv, gain_send, gain_recv, own_sem,
 ):
     ep, tp = lax.axis_index("ep"), lax.axis_index("tp")
-    me, count = ep * count_tp + tp, count_ep * count_tp
     cap, width = picked.shape[1], picked.shape[2]
 
-    def spot(owner):
-        place_rows = pl.ds(pl.multiple_of((owner // count_tp) * cap, cap), cap)
-        place_cols = pl.ds(pl.multiple_of(lax.rem(owner, count_tp) * width, width), width)
+    def spot(owner, owner_tp):
+        place_rows = pl.ds(pl.multiple_of(owner * cap, cap), cap)
+        place_cols = pl.ds(pl.multiple_of(owner_tp * width, width), width)
         return rows_out.at[place_rows, place_cols]
 
     def gain_spot(owner_tp):
@@ -93,11 +89,21 @@
 
     def rows_copy(peer, owner):
         return pltpu.make_async_remote_copy(
-            src_ref=picked.at[peer // count_tp],
-            dst_ref=spot(owner),
+            src_ref=picked.at[peer],
+            dst_ref=spot(owner, tp),
             send_sem=send_sem.at[peer],
             recv_sem=recv_sem.at[owner],
-            device_id=(peer // count_tp, lax.rem(peer, count_tp)),
+            device_id=(peer, tp),
+            device_id_type=MESH,
+        )
+
+    def pass_copy(source, block, peer_tp, owner_tp):
+        return pltpu.make_async_remote_copy(
+            src_ref=source,
+            dst_ref=spot(block, owner_tp),
+            send_sem=pass_send.at[block, peer_tp],
+            recv_sem=pass_recv.at[block, owner_tp],
+            device_id=(ep, peer_tp),
             device_id_type=MESH,
         )
 
@@ -111,27 +117,40 @@
             device_id_type=MESH,
         )
 
-    own_rows = pltpu.make_async_copy(picked.at[ep], spot(me), own_sem.at[0])
+    own_rows = pltpu.make_async_copy(picked.at[ep], spot(ep, tp), own_sem.at[0])
     own_gain = pltpu.make_async_copy(gain, gain_spot(tp), own_sem.at[1])
     own_rows.start()
     own_gain.start()
-    greet_everyone(count, me, count_tp)
-
-    @pl.loop(1, count)
-    def _(step):
-        rows_copy(lax.rem(me + step, count), me).start()
-
-    for step in range(1, count_tp):
-        gain_copy(lax.rem(tp + step, count_tp), tp).start()
+    greet(count_ep, count_tp, ep, tp)
+    for step in range(1, count_ep):
+        rows_copy(lax.rem(ep + step, count_ep), ep).start()
+    for step in range(1, count_tp):
+        peer_tp = lax.rem(tp + step, count_tp)
+        pass_copy(picked.at[ep], ep, peer_tp, tp).start()
+        gain_copy(peer_tp, tp).start()
     own_rows.wait()
     own_gain.wait()
 
-    @pl.loop(1, count)
-    def _(step):
-        peer = lax.rem(me + step, count)
-        copy = rows_copy(peer, peer)
-        copy.wait_send()
-        copy.wait_recv()
+    @pl.loop(1, count_ep)
+    def _(step):
+        block = lax.rem(ep + count_ep - step, count_ep)
+        rows_copy(block, block).wait_recv()
+        for hop in range(1, count_tp):
+            peer_tp = lax.rem(tp + hop, count_tp)
+            pass_copy(spot(block, tp), block, peer_tp, tp).start()
+
+    for step in range(1, count_ep):
+        peer = lax.rem(ep + step, count_ep)
+        rows_copy(peer, peer).wait_send()
+
+    @pl.loop(0, count_ep)
+    def _(step):
+        block = lax.rem(ep + count_ep - step, count_ep)
+        for hop in range(1, count_tp):
+            peer_tp = lax.rem(tp + hop, count_tp)
+            copy = pass_copy(spot(block, tp), block, peer_tp, peer_tp)
+            copy.wait_send()
+            copy.wait_recv()
 
     for step in range(1, count_tp):
         peer_tp = lax.rem(tp + step, count_tp)
@@ -142,7 +161,6 @@
 
 def dispatch(count_ep, count_tp, picked, gain):
     cap, width = picked.shape[1:]
-    count = count_ep * count_tp
     return pl.pallas_call(
         lambda *refs: dispatch_kernel(count_ep, count_tp, *refs),
         out_shape=(
@@ -152,8 +170,10 @@
         in_specs=[pl.BlockSpec(memory_space=pltpu.VMEM)] * 2,
         out_specs=[pl.BlockSpec(memory_space=pltpu.VMEM)] * 2,
         scratch_shapes=[
-            pltpu.SemaphoreType.DMA((count,)),
-            pltpu.SemaphoreType.DMA((count,)),
+            pltpu.SemaphoreType.DMA((count_ep,)),
+            pltpu.SemaphoreType.DMA((count_ep,)),
+            pltpu.SemaphoreType.DMA((count_ep, count_tp)),
+            pltpu.SemaphoreType.DMA((count_ep, count_tp)),
             pltpu.SemaphoreType.DMA((count_tp,)),
             pltpu.SemaphoreType.DMA((count_tp,)),
             pltpu.SemaphoreType.DMA((2,)),
@@ -164,28 +184,35 @@
 
 def return_kernel(
     count_ep, count_tp, partial, first_pick, second_pick, weights, gain, mixed,
-    landed, stats, send_sem, recv_sem, stat_send, stat_recv, own_sem,
+    landed, summed, back, stats,
+    send_sem, recv_sem, part_send, part_recv, stat_send, stat_recv,
 ):
     ep, tp = lax.axis_index("ep"), lax.axis_index("tp")
-    me, count = ep * count_tp + tp, count_ep * count_tp
     cap, width = partial.shape[0] // count_ep, partial.shape[1] // count_tp
 
-    def source(owner):
-        from_rows = pl.ds(pl.multiple_of((owner // count_tp) * cap, cap), cap)
-        from_cols = pl.ds(pl.multiple_of(lax.rem(owner, count_tp) * width, width), width)
-        return partial.at[from_rows, from_cols]
-
-    def spot(owner):
-        place_rows = pl.ds(pl.multiple_of((owner // count_tp) * cap, cap), cap)
-        return landed.at[lax.rem(owner, count_tp), place_rows, :]
-
-    def rows_copy(peer, owner):
-        return pltpu.make_async_remote_copy(
-            src_ref=source(peer),
-            dst_ref=spot(owner),
+    def block_rows(block):
+        return pl.ds(pl.multiple_of(block * cap, cap), cap)
+
+    def part_cols(part):
+        return pl.ds(pl.multiple_of(part * width, width), width)
+
+    def part_copy(block, peer_tp, owner_tp):
+        return pltpu.make_async_remote_copy(
+            src_ref=partial.at[block_rows(block), part_cols(peer_tp)],
+            dst_ref=landed.at[owner_tp, block_rows(block), :],
+            send_sem=part_send.at[block, peer_tp],
+            recv_sem=part_recv.at[block, owner_tp],
+            device_id=(ep, peer_tp),
+            device_id_type=MESH,
+        )
+
+    def back_copy(peer, owner):
+        return pltpu.make_async_remote_copy(
+            src_ref=summed.at[block_rows(peer), :],
+            dst_ref=back.at[block_rows(owner), :],
             send_sem=send_sem.at[peer],
             recv_sem=recv_sem.at[owner],
-            device_id=(peer // count_tp, lax.rem(peer, count_tp)),
+            device_id=(peer, tp),
             device_id_type=MESH,
         )
 
@@ -199,30 +226,48 @@
             device_id_type=MESH,
         )
 
-    own_rows = pltpu.make_async_copy(source(me), spot(me), own_sem.at[0])
-    own_rows.start()
-    greet_everyone(count, me, count_tp)
-
-    @pl.loop(1, count)
-    def _(step):
-        rows_copy(lax.rem(me + step, count), me).start()
-
-    own_rows.wait()
-
-    @pl.loop(1, count)
-    def _(step):
-        peer = lax.rem(me + step, count)
-        copy = rows_copy(peer, peer)
+    def block_sum(block):
+        total = partial[block_rows(block), part_cols(tp)].astype(jnp.float32)
+        for hop in range(1, count_tp):
+            peer_tp = lax.rem(tp + hop, count_tp)
+            part_copy(block, peer_tp, peer_tp).wait_recv()
+            total += landed[peer_tp, block_rows(block), :].astype(jnp.float32)
+        return total.astype(jnp.bfloat16)
+
+    greet(count_ep, count_tp, ep, tp)
+
+    @pl.loop(1, count_ep + 1)
+    def _(step):
+        block = lax.rem(ep + step, count_ep)
+        for hop in range(1, count_tp):
+            part_copy(block, lax.rem(tp + hop, count_tp), tp).start()
+
+    @pl.loop(1, count_ep)
+    def _(step):
+        block = lax.rem(ep + step, count_ep)
+        summed[block_rows(block), :] = block_sum(block)
+        back_copy(block, ep).start()
+
+    back[block_rows(ep), :] = block_sum(ep)
+
+    @pl.loop(1, count_ep)
+    def _(step):
+        peer = lax.rem(ep + count_ep - step, count_ep)
+        copy = back_copy(peer, peer)
         copy.wait_send()
         copy.wait_recv()
 
-    def picked_sum(pick):
-        total = jnp.zeros(mixed.shape, jnp.float32)
-        for part in range(count_tp):
-            total += jnp.dot(pick[...], landed[part], preferred_element_type=jnp.float32)
-        return total
-
-    combined = weights[:, 0:1] * picked_sum(first_pick) + weights[:, 1:2] * picked_sum(second_pick)
+    @pl.loop(0, count_ep)
+    def _(block):
+        for hop in range(1, count_tp):
+            part_copy(block, lax.rem(tp + hop, count_tp), tp).wait_send()
+
+    returned = back[...]
+    combined = weights[:, 0:1] * jnp.dot(
+        first_pick[...], returned, preferred_element_type=jnp.float32
+    ) + weights[:, 1:2] * jnp.dot(
+        second_pick[...], returned, preferred_element_type=jnp.float32
+    )
     squares = jnp.sum(combined * combined, axis=1, keepdims=True)
     stats[tp] = jnp.broadcast_to(squares, stats.shape[1:])
     for step in range(1, count_tp):
@@ -241,7 +286,6 @@
 
 def give_back(count_ep, count_tp, partial, picks, weights, gain):
     tok_rows, width = weights.shape[0], gain.shape[1]
-    count = count_ep * count_tp
     return pl.pallas_call(
         lambda *refs: return_kernel(count_ep, count_tp, *refs),
         out_shape=jax.ShapeDtypeStruct((tok_rows, width), jnp.bfloat16),
@@ -249,12 +293,15 @@
         out_specs=pl.BlockSpec(memory_space=pltpu.VMEM),
         scratch_shapes=[
             pltpu.VMEM((count_tp, partial.shape[0], width), jnp.bfloat16),
+            pltpu.VMEM((partial.shape[0], width), jnp.bfloat16),
+            pltpu.VMEM((partial.shape[0], width), jnp.bfloat16),
             pltpu.VMEM((count_tp, tok_rows, 128), jnp.float32),
-            pltpu.SemaphoreType.DMA((count,)),
-            pltpu.SemaphoreType.DMA((count,)),
+            pltpu.SemaphoreType.DMA((count_ep,)),
+            pltpu.SemaphoreType.DMA((count_ep,)),
+            pltpu.SemaphoreType.DMA((count_ep, count_tp)),
+            pltpu.SemaphoreType.DMA((count_ep, count_tp)),
             pltpu.SemaphoreType.DMA((count_tp,)),
             pltpu.SemaphoreType.DMA((count_tp,)),
-            pltpu.SemaphoreType.DMA((1,)),
         ],
         compiler_params=pltpu.CompilerParams(collective_id=1, has_side_effects=True),
     )(partial, picks[0], picks[1], weights, gain)

time: 153 us -> 110 us (0.72)
  the two profiles are of different devices: /device:TPU:9 before, /device:TPU:0 now
where the time goes in v2:
time: 110 us
  Pallas kernels  70.6 us (64%)
  matrix products  29.4 us (27%)
  other arithmetic  5.01 us (5%)
  local copies, waits for them, and re-layouts  4.45 us (4%)
    pallas_call x1, Pallas kernels, give_back(): pl.pallas_call(lambda *refs: return_kernel(count_ep, count_tp, *refs), ou...  36.5 us
    pallas_call x1, Pallas kernels, dispatch(): pl.pallas_call(lambda *refs: dispatch_kernel(count_ep, count_tp, *refs),...  34.1 us
    dot_general x1, matrix products, on_device_direct(): jnp.dot(hidden, w_down[0], preferred_element_type=jnp.float32)  17.6 us
    dot_general x1, matrix products, on_device_direct(): gate_part = jnp.dot(normed, w_gate[0], preferred_element_type=jnp.float32)  10.6 us
    unnamed x8, local copies, waits for them, and re-layouts  2.31 us

profile of v2, /device:TPU:0, one launch (start us, length us, event | category | flops | bytes accessed | tf_op | source)
XLA Modules:
  0.0 109.5 jit_solution(6892761781430477024)
XLA Ops:
  0.0 0.0 copy-start
  0.0 0.7 convert_reduce_fusion
  0.7 0.1 fusion.28
  0.9 0.7 select_reduce_fusion
  1.6 0.7 convert_add_fusion
  2.3 0.0 copy-done
  2.3 1.1 convolution_convert_fusion
  3.4 1.3 %broadcast_in_dim.4.refs_1_ = f32[8,512]{1,0:T(8,128)} broadcast(f32[512]{0:T(512)} %param.11), dimensions={1} | broadcast | bytes 18432 | tf_op jit(solution)/shard_map/broadcast_in_dim | solution.py:337
  4.6 34.1 %shard_map.82 = (bf16[512,2048]{1,0:T(8,128)(2,1)}, f32[8,2048]{1,0:T(8,128)}) custom-call(bf16[8,64,512]{2,1,0:T(8,128)(2,1)} %bitcast.26, f32[8,512]{1,0:T(8,128)} %broadcast_in_dim.4.refs_1_), custom_call_target="tpu_custom_call" | custom-call | tf_op jit(solution)/shard_map/pallas_call | solution.py:164
  38.8 2.1 %fusion.6 = f32[512]{0:T(512)S(1)} fusion(bf16[512,2048]{1,0:T(8,128)(2,1)} %get-tuple-element.7), kind=kLoop, calls=%fused_computation.8 | loop fusion | flops 3145216 | bytes 2099200 | tf_op jit(solution)/shard_map/reduce_sum | solution.py:340
  40.9 0.9 slice.13
  41.7 0.0 copy-start.1
  41.7 10.6 %fusion.4 = f32[512,2048]{1,0:T(8,128)} fusion(bf16[1,2048,2048]{2,1,0:T(8,128)(2,1)} %param.13, bf16[512,2048]{1,0:T(8,128)(2,1)} %get-tuple-element.7, f32[2048]{0:T(1024)S(1)} %bitcast.27, f32[512]{0:T(512)S(1)} %add_rsqrt_fusion), kind=kOutput, calls=%fused_computation.4 | convolution fusion | flops 4299161600 | bytes 14690304 | tf_op jit(solution)/shard_map/dot_general | solution.py:344
  52.3 0.0 copy-done.1
  52.3 0.0 copy-start.2
  52.4 17.6 %fusion.13.refs_0_ = bf16[512,2048]{1,0:T(8,128)(2,1)} fusion(bf16[1,2048,2048]{2,1,0:T(8,128)(2,1)} %param.15, f32[512,2048]{1,0:T(8,128)} %fusion.4, bf16[1,2048,2048]{2,1,0:T(8,128)(2,1)} %param.14, bf16[512,2048]{1,0:T(8,128)(2,1)S(1)} %copy-done.1, f32[2048]{0:T(1024)S(1)} %bitcast.28, f32[512]{0:T(512)S(1)} %add_rsqrt_fusion), kind=kOutput, calls=%fused_computation.12 | convolution fusion | flops 8601468928 | bytes 25176064 | tf_op jit(solution)/shard_map/dot_general | solution.py:347
  69.9 0.8 fusion.24
  70.7 0.0 copy-done.2
  70.7 0.7 copy.12.refs_3_
  71.5 36.5 %shard_map.83 = bf16[128,512]{1,0:T(8,128)(2,1)} custom-call(bf16[512,2048]{1,0:T(8,128)(2,1)} %fusion.13.refs_0_, bf16[128,512]{1,0:T(8,128)(2,1)} %get-tuple-element.11.refs_1_, bf16[128,512]{1,0:T(8,128)(2,1)} %get-tuple-element.12.refs_2_, f32[128,2]{1,0:T(8,128)} %copy.12.refs_3_, f32[1,512]{1,0:T(1,128)} %bitcast.29), custom_call_target="tpu_custom_call" | custom-call | tf_op jit(solution)/shard_map/pallas_call | solution.py:289
  107.9 1.6 %copy.14 = bf16[128,512]{1,0:T(8,128)(2,1)} copy(bf16[128,512]{1,0:T(8,128)(2,1)} %shard_map.83) | data formatting | bytes 262144
  (2 shorter events, 0.0 us)
Async XLA Ops:
  0.0 2.3 %copy-start = (bf16[128,512]{1,0:T(8,128)(2,1)S(1)}, bf16[128,512]{1,0:T(8,128)(2,1)}, u32[]{:S(2)}) copy-start(bf16[128,512]{1,0:T(8,128)(2,1)} %param.8) | copy-start | bytes 393220
  41.7 10.6 %copy-start.1 = (bf16[512,2048]{1,0:T(8,128)(2,1)S(1)}, bf16[512,2048]{1,0:T(8,128)(2,1)}, u32[]{:S(2)}) copy-start(bf16[512,2048]{1,0:T(8,128)(2,1)} %get-tuple-element.7) | copy-start | bytes 6291460
  52.3 18.4 %copy-start.2 = (f32[128,2]{0,1:T(2,128)S(1)}, f32[128,2]{0,1:T(2,128)}, u32[]{:S(2)}) copy-start(f32[128,2]{0,1:T(2,128)} %param.10) | copy-start | bytes 3076
